TPU v7x, 32 devices: a whole 2x2x4 slice. The times are simulated.
32 devices in a mesh: sp: 4 (over z), tp: 4 (over y, x), dp: 2 (over core).
Axes of the slice: x: 2, y: 2, z: 4, core: 2. Of those that a mesh axis runs over, the one named last changes fastest.
Arguments:
- latent: bfloat16 [2, 1024, 2048], P('dp', ('sp', 'tp')), may hold values from -6 to 6
- condition: bfloat16 [2, 2048], P('dp', ('sp', 'tp')), may hold values from -6 to 6
- context: bfloat16 [2, 32, 2048], P('dp', 'sp'), may hold values from -6 to 6
- context_vector: bfloat16 [2048], P(('sp', 'tp')), may hold values from -6 to 6
- modulator: bfloat16 [2048, 6144], P(('sp', 'tp')), may hold values from -0.3125 to 0.3125
- norm_gain: float32 [2048], replicated, may hold values from 0.1 to 1.9
- query_weight: bfloat16 [2048, 512], P(None, 'tp'), may hold values from -4 to 4
- key_weight: bfloat16 [2048, 512], P(None, 'tp'), may hold values from -0.125 to 0.125
- value_weight: bfloat16 [2048, 512], P(None, 'tp'), may hold values from -0.125 to 0.125
- head_gain: float32 [128], replicated, may hold values from 0.1 to 1.9
- lambdas: float32 [4], P('tp'), may hold values from 0.3 to 0.8
- context_bias: float32 [4, 2], P('tp'), may hold values from 1.3 to 2.7
- out_weight: bfloat16 [512, 2048], P('tp'), may hold values from -0.25 to 0.25
Outputs:
- updated: bfloat16 [2, 1024, 2048], P('dp', ('sp', 'tp'))
All inputs are finite; a program needn't handle non-finite values.
Results may differ from a plain program's by a relative error of at most 0.024.
Values may be sent and summed in bfloat16 or wider, within the bound.
A program may use at most 64 MiB of HBM per device.

v0:
```python
import functools

import jax
import jax.numpy as jnp
from jax import lax
from jax.experimental import pallas as pl
from jax.experimental.pallas import tpu as pltpu
from jax.sharding import PartitionSpec as P

EPSILON = 1e-06
OUT_SCALE = 0.8
KEY_BLOCK = 2048
LOW_START = -1e30


def modulate(inputs, gain_vector, shift_vector, scale_vector):
    as_float = inputs.astype(jnp.float32)
    normed = as_float * lax.rsqrt(jnp.mean(as_float * as_float, axis=-1, keepdims=True) + EPSILON)
    return (normed * gain_vector * (1.0 + scale_vector) + shift_vector).astype(jnp.bfloat16)


def fold_block(running, queries, keys_in, values_in, key_flags, bias_table, score_scale):
    run_max, run_total, summed = running
    scores = (
        jnp.einsum("qhmd,khmd->hmqk", queries, keys_in, preferred_element_type=jnp.float32)
        * score_scale
    )
    if key_flags is not None:
        scores = scores + bias_table[:, :, None, None] * key_flags
    new_max = jnp.maximum(run_max, jnp.max(scores, axis=-1))
    shrink = jnp.exp(run_max - new_max)
    weights = jnp.exp(scores - new_max[..., None])
    run_total = run_total * shrink + jnp.sum(weights, axis=-1)
    summed = summed * shrink[..., None] + jnp.einsum(
        "hmqk,khe->hmqe",
        weights.astype(jnp.bfloat16),
        values_in,
        preferred_element_type=jnp.float32,
    )
    return (new_max, run_total, summed)


def fold_keys(running, queries, keys_in, values_in, key_flags, bias_table, score_scale):
    full_blocks = keys_in.shape[0] // KEY_BLOCK
    if full_blocks > 1:
        edge = full_blocks * KEY_BLOCK
        stacked = (
            keys_in[:edge].reshape((full_blocks, KEY_BLOCK) + keys_in.shape[1:]),
            values_in[:edge].reshape((full_blocks, KEY_BLOCK) + values_in.shape[1:]),
        )
        if key_flags is not None:
            stacked = stacked + (key_flags[:edge].reshape(full_blocks, KEY_BLOCK),)

        def fold_step(current, block_data):
            flag_part = None if key_flags is None else block_data[2]
            return (
                fold_block(
                    current,
                    queries,
                    block_data[0],
                    block_data[1],
                    flag_part,
                    bias_table,
                    score_scale,
                ),
                None,
            )

        running, ignored = lax.scan(fold_step, running, stacked)
        keys_in = keys_in[edge:]
        values_in = values_in[edge:]
        key_flags = None if key_flags is None else key_flags[edge:]
    if keys_in.shape[0] > 0:
        running = fold_block(
            running, queries, keys_in, values_in, key_flags, bias_table, score_scale
        )
    return running


def body(
    latent,
    condition,
    context,
    context_vector,
    modulator,
    norm_gain,
    query_weight,
    key_weight,
    value_weight,
    head_gain,
    lambdas,
    context_bias,
    out_weight,
):
    model_width = latent.shape[2]
    local_heads = lambdas.shape[0]
    query_width = query_weight.shape[1]
    head_size = query_width // (2 * local_heads)
    value_size = value_weight.shape[1] // local_heads
    score_scale = head_size ** (-0.5)
    activated = jax.nn.silu(
        jnp.concatenate([condition, context_vector[None, :]], axis=0).astype(jnp.float32)
    )
    partial_terms = jnp.dot(
        activated.astype(jnp.bfloat16), modulator, preferred_element_type=jnp.float32
    )
    modulations = lax.psum(partial_terms, ("sp", "tp"))
    hidden = modulate(
        latent[0],
        norm_gain,
        modulations[0, :model_width],
        modulations[0, model_width : 2 * model_width],
    )
    ctx_hidden = modulate(
        context[0],
        norm_gain,
        modulations[1, :model_width],
        modulations[1, model_width : 2 * model_width],
    )
    gate_vector = modulations[0, 2 * model_width :]
    incoming = lax.all_gather(hidden, "tp", axis=0, tiled=True)
    projected = jnp.concatenate(
        [
            jnp.dot(incoming, query_weight, preferred_element_type=jnp.float32),
            jnp.dot(incoming, key_weight, preferred_element_type=jnp.float32),
            jnp.dot(incoming, value_weight, preferred_element_type=jnp.float32),
        ],
        axis=1,
    ).astype(jnp.bfloat16)
    query_rows = projected.shape[0]
    queries = projected[:, :query_width].reshape(query_rows, local_heads, 2, head_size)
    own_keys = projected[:, query_width : 2 * query_width]
    own_values = projected[:, 2 * query_width :]
    gathered_context = lax.all_gather(ctx_hidden, "sp", axis=0, tiled=True)
    ctx_keys = jnp.dot(gathered_context, key_weight, preferred_element_type=jnp.float32).astype(
        jnp.bfloat16
    )
    ctx_values = jnp.dot(gathered_context, value_weight, preferred_element_type=jnp.float32).astype(
        jnp.bfloat16
    )
    start_carry = (
        jnp.full((local_heads, 2, query_rows), LOW_START, jnp.float32),
        jnp.zeros((local_heads, 2, query_rows), jnp.float32),
        jnp.zeros((local_heads, 2, query_rows, value_size), jnp.float32),
    )
    pieces = (own_keys, own_values)
    initial = fold_keys(
        start_carry,
        queries,
        ctx_keys.reshape(-1, local_heads, 2, head_size),
        ctx_values.reshape(-1, local_heads, value_size),
        jnp.ones((ctx_keys.shape[0],), jnp.float32),
        context_bias,
        score_scale,
    )
    incoming = (
        lax.all_gather(pieces[0], "sp", axis=0, tiled=True),
        lax.all_gather(pieces[1], "sp", axis=0, tiled=True),
    )
    run_max, run_total, summed = fold_keys(
        initial,
        queries,
        incoming[0].reshape(-1, local_heads, 2, head_size),
        incoming[1].reshape(-1, local_heads, value_size),
        None,
        context_bias,
        score_scale,
    )
    mixed = (
        summed[:, 0] / run_total[:, 0, :, None]
        - lambdas[:, None, None] * summed[:, 1] / run_total[:, 1, :, None]
    )
    normed = (
        mixed
        * lax.rsqrt(jnp.mean(mixed * mixed, axis=-1, keepdims=True) + EPSILON)
        * head_gain
        * OUT_SCALE
    )
    attended = (
        jnp.transpose(normed, (1, 0, 2))
        .reshape(query_rows, local_heads * value_size)
        .astype(jnp.bfloat16)
    )
    exchanged = lax.all_to_all(attended, "tp", split_axis=0, concat_axis=1, tiled=True)
    whole_weight = lax.all_gather(out_weight, "tp", axis=0, tiled=True)
    branch = jnp.dot(exchanged, whole_weight, preferred_element_type=jnp.float32)
    result = (latent[0].astype(jnp.float32) + gate_vector * branch).astype(jnp.bfloat16)
    return result[None]


MESH = pl.DeviceIdType.MESH
LANES = 128


class Phases:
    def __init__(self):
        self.open = None

    def __call__(self, name):
        if self.open is not None:
            self.open.__exit__(None, None, None)
        self.open = None
        if name is not None:
            self.open = jax.named_scope(name)
            self.open.__enter__()


def fused_kernel(
    sp_n, tp_n, score_scale,
    latent, condition_in, context, vector_in, modulator, gain_in,
    query_weight, key_weight, value_weight, head_gain_in, lambdas_in, bias_in, out_weight,
    out,
    condition, context_vector, norm_gain, head_gain, lambdas, context_bias,
    mod_v, part, rs_in, mods, lat, ctx_all, w_q, w_kv, w_out, vecs, hid, kvb, att_out, att_in,
    small_sem, own_sem, rs_ss, rs_rs, ag_ss, ag_rs, lat_ss, lat_rs, ctx_ss, ctx_rs,
    kv_os, kv_ss, kv_rs, wt_ss, wt_rs, wd_ss, wd_rs, at_ss, at_rs,
):
    sp = lax.axis_index("sp")
    tp = lax.axis_index("tp")
    dp = lax.axis_index("dp")
    n = sp_n * tp_n
    rank = sp * tp_n + tp
    across = tp + 1 - 2 * lax.rem(tp, 2)
    along = lax.rem(tp + 2, 4)
    corner = along + 1 - 2 * lax.rem(along, 2)
    roles = (tp, across, along, corner)
    half = lat.shape[1]
    width = lat.shape[2]
    rows = half * 2
    qrows = rows * tp_n
    chunk = part.shape[2]

    phase = Phases()
    phase("enter")
    barrier = pltpu.get_barrier_semaphore()

    small = [
        pltpu.make_async_copy(source, place, small_sem.at[k])
        for k, (source, place) in enumerate((
            (condition_in, condition), (vector_in, context_vector), (context, ctx_all.at[sp]),
            (gain_in, norm_gain), (head_gain_in, head_gain), (lambdas_in, lambdas),
            (bias_in, context_bias),
        ))
    ]
    loads = [
        pltpu.make_async_copy(modulator, mod_v, own_sem.at[0]),
        pltpu.make_async_copy(latent, lat.at[pl.ds(tp * 2, 2)], own_sem.at[1]),
        pltpu.make_async_copy(key_weight, w_kv.at[:, pl.ds(0, LANES)], own_sem.at[2]),
        pltpu.make_async_copy(value_weight, w_kv.at[:, pl.ds(LANES, LANES)], own_sem.at[3]),
        pltpu.make_async_copy(query_weight, w_q, own_sem.at[4]),
        pltpu.make_async_copy(out_weight, w_out.at[pl.ds(tp * 4, 4)], own_sem.at[5]),
    ]
    for load in small[:2] + loads[:2] + small[2:] + loads[2:]:
        load.start()

    def greet(d, carry):
        peer = lax.rem(rank + d, n)
        pl.semaphore_signal(
            barrier, inc=1, device_id=(peer // tp_n, lax.rem(peer, tp_n), dp), device_id_type=MESH
        )
        return carry

    lax.fori_loop(1, n, greet, 0)
    pl.semaphore_signal(barrier, inc=1, device_id=(sp, tp, 1 - dp), device_id_type=MESH)

    phase("partial")
    for load in small:
        load.wait()
    rows_in = jnp.concatenate([condition[...], context_vector[...]], axis=0).astype(jnp.float32)
    activated = jax.nn.silu(rows_in).astype(jnp.bfloat16)
    loads[0].wait()
    partial_terms = jnp.dot(activated, mod_v[...], preferred_element_type=jnp.float32)
    for p in range(n):
        part[p] = partial_terms[:, p * chunk : (p + 1) * chunk]
    loads[1].wait()
    phase("barrier")
    pl.semaphore_wait(barrier, n)
    phase("sends")

    def rs_copy(d):
        peer = lax.rem(rank + d, n)
        return pltpu.make_async_remote_copy(
            src_ref=part.at[peer], dst_ref=rs_in.at[d], send_sem=rs_ss.at[0], recv_sem=rs_rs.at[0],
            device_id=(peer // tp_n, lax.rem(peer, tp_n), dp), device_id_type=MESH,
        )

    def ag_copy(d):
        peer = lax.rem(rank + d, n)
        return pltpu.make_async_remote_copy(
            src_ref=mods.at[rank], dst_ref=mods.at[rank], send_sem=ag_ss.at[0], recv_sem=ag_rs.at[0],
            device_id=(peer // tp_n, lax.rem(peer, tp_n), dp), device_id_type=MESH,
        )

    def rs_all():
        return pltpu.make_async_remote_copy(
            src_ref=part.at[pl.ds(0, n - 1)], dst_ref=rs_in.at[pl.ds(1, n - 1)],
            send_sem=rs_ss.at[0], recv_sem=rs_rs.at[0],
            device_id=(sp, across, dp), device_id_type=MESH,
        )

    def ag_all():
        return pltpu.make_async_remote_copy(
            src_ref=mods.at[pl.ds(0, n - 1)], dst_ref=mods.at[pl.ds(0, n - 1)],
            send_sem=ag_ss.at[0], recv_sem=ag_rs.at[0],
            device_id=(sp, across, dp), device_id_type=MESH,
        )

    def each(first, last, act):
        def step(d, carry):
            act(d)
            return carry

        lax.fori_loop(first, last, step, 0)

    each(1, n, lambda d: rs_copy(d).start())


    class Plane:
        def __init__(self, buf, index, ss, rs):
            self.buf, self.index, self.ss, self.rs = buf, index, ss, rs

        def copy(self, owner, part_no, target, slot, kind):
            place = self.buf.at[self.index(owner, part_no)]
            return pltpu.make_async_remote_copy(
                src_ref=place, dst_ref=place, send_sem=self.ss.at[slot],
                recv_sem=self.rs.at[kind * 2 + part_no],
                device_id=(sp, target, dp), device_id_type=MESH,
            )

        def first(self):
            return [
                self.copy(tp, 0, across, 0, 0),
                self.copy(tp, 1, along, 1, 1),
                self.copy(tp, 1, across, 2, 0),
                self.copy(tp, 0, along, 3, 1),
            ]

        def relays(self):
            return [self.copy(across, 0, along, 4, 2), self.copy(along, 1, across, 5, 2)]

        def arrival(self, kind, part_no):
            owner = (across, along, corner)[kind]
            return self.copy(owner, part_no, across, 0, kind)

    plane = Plane(lat, lambda o, q: o * 2 + q, lat_ss, lat_rs)
    lat_first = plane.first()
    for copy in lat_first:
        copy.start()

    def ctx_copy(d):
        peer = lax.rem(sp + d, sp_n)
        return pltpu.make_async_remote_copy(
            src_ref=ctx_all.at[sp], dst_ref=ctx_all.at[sp], send_sem=ctx_ss.at[d], recv_sem=ctx_rs.at[d],
            device_id=(peer, tp, dp), device_id_type=MESH,
        )

    def ctx_arrival(d):
        peer = lax.rem(sp - d + sp_n, sp_n)
        return pltpu.make_async_remote_copy(
            src_ref=ctx_all.at[peer], dst_ref=ctx_all.at[peer], send_sem=ctx_ss.at[d], recv_sem=ctx_rs.at[d],
            device_id=(peer, tp, dp), device_id_type=MESH,
        )

    for d in range(1, sp_n):
        ctx_copy(d).start()
    rs_in[0] = part[rank]

    phase("rs_wait")
    rs_all().wait_recv()
    total = rs_in[0]
    for d in range(1, n):
        total = total + rs_in[d]
    mods[rank] = total
    each(1, n, lambda d: ag_copy(d).start())

    phase("lat_relay")
    lat_relays = plane.relays()
    plane.arrival(0, 0).wait_recv()
    lat_relays[0].start()
    plane.arrival(1, 1).wait_recv()
    lat_relays[1].start()

    loads[5].wait()
    wplane = Plane(w_out, lambda o, q: o * 4 + dp * 2 + q, wt_ss, wt_rs)
    w_first = wplane.first()
    for copy in w_first:
        copy.start()

    for d in range(1, sp_n):
        ctx_arrival(d).wait_recv()
    phase("ag_wait")
    ag_all().wait_recv()
    whole = jnp.concatenate([mods[p] for p in range(n)], axis=1)
    phase("vecs")
    gain = norm_gain[...]
    vecs[0:1, :] = gain * (1.0 + whole[0:1, width : 2 * width])
    vecs[1:2, :] = whole[0:1, :width]
    vecs[2:3, :] = gain * (1.0 + whole[1:2, width : 2 * width])
    vecs[3:4, :] = whole[1:2, :width]
    vecs[4:5, :] = whole[0:1, 2 * width :]

    def normed_rows(x, at):
        x = x.astype(jnp.float32)
        scale = lax.rsqrt(jnp.mean(x * x, axis=-1, keepdims=True) + EPSILON)
        return (x * scale * vecs[at : at + 1, :] + vecs[at + 1 : at + 2, :]).astype(jnp.bfloat16)

    def norm_block(role):
        for q in range(2):
            at = (role * 2 + q) * half
            hid[at : at + half, :] = normed_rows(lat[roles[role] * 2 + q], 0)

    def kv_own(to, slot, q):
        place = kvb.at[sp * 2 + q]
        return pltpu.make_async_remote_copy(
            src_ref=place, dst_ref=place, send_sem=kv_os.at[slot * 2 + q],
            recv_sem=kv_rs.at[sp * 2 + q], device_id=(to, tp, dp), device_id_type=MESH,
        )

    def kv_rows(first, last):
        product = jnp.dot(hid[first:last, :], w_kv[...], preferred_element_type=jnp.float32)
        return product.astype(jnp.bfloat16)

    def kv_send(q):
        pl.when(sp + 1 < sp_n)(lambda: kv_own(sp + 1, 0, q).start())
        pl.when(sp > 0)(lambda: kv_own(sp - 1, 1, q).start())

    piece = qrows // 2
    ctx_rows = ctx_all.shape[0] * ctx_all.shape[1]
    norm_block(0)
    plane.arrival(0, 1).wait_recv()
    norm_block(1)
    phase("kv0")
    for load in loads[2:5]:
        load.wait()
    kv_near = kv_rows(0, piece)
    kvb[sp * 2] = kv_near
    kv_send(0)
    phase("lat_rest")
    hid[qrows : qrows + ctx_rows, :] = normed_rows(
        ctx_all[...].astype(jnp.float32).reshape(ctx_rows, width), 2
    )
    plane.arrival(1, 0).wait_recv()
    norm_block(2)
    plane.arrival(2, 0).wait_recv()
    plane.arrival(2, 1).wait_recv()
    norm_block(3)
    phase("kv1")
    kv_far = kv_rows(piece, qrows + ctx_rows)
    kvb[sp * 2 + 1] = kv_far[:piece]
    kv_send(1)
    kv = jnp.concatenate([kv_near, kv_far[:piece]], axis=0)
    ctx_kv = kv_far[piece:]

    phase("queries")
    queries = jnp.dot(hid[:qrows, :], w_q[...], preferred_element_type=jnp.float32) * score_scale
    queries = queries.astype(jnp.bfloat16)
    head = queries.shape[1] // 2
    lane = lax.broadcasted_iota(jnp.int32, queries.shape, 1)
    zero = jnp.zeros_like(queries)
    both = jnp.concatenate(
        [jnp.where(lane < head, queries, zero), jnp.where(lane < head, zero, queries)], axis=0
    )

    def score(keys):
        return lax.dot_general(
            both, keys, (((1,), (1,)), ((), ())), preferred_element_type=jnp.float32
        )

    map_row = lax.broadcasted_iota(jnp.int32, (2 * qrows, 1), 0)
    bias = jnp.where(map_row < qrows, context_bias[0:1, 0:1], context_bias[0:1, 1:2])

    def fold(running, scores, values):
        top = jnp.max(scores, axis=-1, keepdims=True)
        if running is not None:
            top = jnp.maximum(running[0], top)
        weights = jnp.exp(scores - top)
        count = jnp.sum(weights, axis=-1, keepdims=True)
        summed = jnp.dot(weights.astype(jnp.bfloat16), values, preferred_element_type=jnp.float32)
        if running is not None:
            shrink = jnp.exp(running[0] - top)
            count = running[1] * shrink + count
            summed = running[2] * shrink + summed
        return top, count, summed

    phase("fold_own")
    running = fold(None, score(ctx_kv[:, :LANES]) + bias, ctx_kv[:, LANES:])
    running = fold(running, score(kv[:, :LANES]), kv[:, LANES:])

    def sibling(owner, part_no, slot):
        place = w_out.at[owner * 4 + dp * 2 + part_no]
        return pltpu.make_async_remote_copy(
            src_ref=place, dst_ref=place, send_sem=wd_ss.at[slot], recv_sem=wd_rs.at[slot],
            device_id=(sp, tp, 1 - dp), device_id_type=MESH,
        )

    def sibling_arrival(owner, part_no, slot):
        place = w_out.at[owner * 4 + (1 - dp) * 2 + part_no]
        return pltpu.make_async_remote_copy(
            src_ref=place, dst_ref=place, send_sem=wd_ss.at[slot], recv_sem=wd_rs.at[slot],
            device_id=(sp, tp, 1 - dp), device_id_type=MESH,
        )

    owners = (across, along, corner)
    w_sent = []

    def swap(kind, part_no, wait=True):
        if wait:
            wplane.arrival(kind, part_no).wait_recv()
        copy = sibling(owners[kind], part_no, kind * 2 + part_no)
        copy.start()
        w_sent.append(copy)

    high = (2 * sp) // sp_n

    def block_at(t):
        up = (t - 1) + jnp.where(t - 1 >= sp, 1, 0)
        down = (sp_n - t) - jnp.where(sp_n - t <= sp, 1, 0)
        return jnp.where(high == 0, up, down)

    def onward(b, q):
        step = jnp.where(b < sp, 1, -1)
        to = sp + step
        ok = jnp.logical_and(to >= 0, to < sp_n)
        safe = jnp.where(ok, to, sp - step)
        return ok, pltpu.make_async_remote_copy(
            src_ref=kvb.at[b * 2 + q], dst_ref=kvb.at[b * 2 + q], send_sem=kv_ss.at[b * 2 + q],
            recv_sem=kv_rs.at[b * 2 + q], device_id=(safe, tp, dp), device_id_type=MESH,
        )

    sent = []
    def take(t, q):
        ok, copy = onward(block_at(t), q)
        copy.wait_recv()
        pl.when(ok)(copy.start)
        sent.append((ok, copy))

    near = [t for t in (1, 2) if t < sp_n]
    phase("take_near")
    for t in near:
        take(t, 0)
    phase("w_relay")
    w_relays = wplane.relays()
    wplane.arrival(0, 0).wait_recv()
    w_relays[0].start()
    wplane.arrival(1, 1).wait_recv()
    w_relays[1].start()
    swap(0, 0, False)
    swap(1, 1, False)

    phase("take_near2")
    for t in near:
        take(t, 1)
    swap(0, 1)
    swap(1, 0)
    phase("fold_near")
    for t in near:
        block = kvb[pl.ds(block_at(t) * 2, 2)].reshape(qrows, 2 * LANES)
        running = fold(running, score(block[:, :LANES]), block[:, LANES:])
    for t in range(3, sp_n):
        for q in range(2):
            phase(f"take{t}_{q}")
            take(t, q)
            block = kvb[block_at(t) * 2 + q]
            running = fold(running, score(block[:, :LANES]), block[:, LANES:])

    phase("finish")
    top, count, summed = running
    shares = summed / count
    mixed = shares[:qrows] - lambdas[...] * shares[qrows:]
    normed = (
        mixed
        * lax.rsqrt(jnp.mean(mixed * mixed, axis=-1, keepdims=True) + EPSILON)
        * head_gain[...]
        * OUT_SCALE
    ).astype(jnp.bfloat16)
    for p in range(tp_n):
        att_out[p] = normed[p * rows : (p + 1) * rows]

    def at_copy(d):
        return pltpu.make_async_remote_copy(
            src_ref=att_out.at[d], dst_ref=att_in.at[tp], send_sem=at_ss.at[d], recv_sem=at_rs.at[d],
            device_id=(sp, roles[d], dp), device_id_type=MESH,
        )

    def at_arrival(d):
        return pltpu.make_async_remote_copy(
            src_ref=att_out.at[d], dst_ref=att_in.at[roles[d]], send_sem=at_ss.at[d],
            recv_sem=at_rs.at[d], device_id=(sp, roles[d], dp), device_id_type=MESH,
        )

    for d in (3, 1, 2):
        at_copy(d).start()
    att_in[tp] = att_out[0]

    phase("w_wait")
    swap(2, 0)
    swap(2, 1)
    for kind in range(3):
        for part_no in range(2):
            sibling_arrival(owners[kind], part_no, kind * 2 + part_no).wait_recv()
    phase("at_wait")
    for d in range(1, tp_n):
        at_arrival(d).wait_recv()

    phase("out")
    attended = jnp.concatenate([att_in[p] for p in range(tp_n)], axis=1)
    step = 512
    for first in range(0, width, step):
        cols = slice(first, first + step)
        weight = w_out[:, :, cols].reshape(attended.shape[1], step)
        branch = jnp.dot(attended, weight, preferred_element_type=jnp.float32)
        for q in range(2):
            mine = lat[tp * 2 + q, :, cols].astype(jnp.float32)
            update = mine + vecs[4:5, cols] * branch[q * half : (q + 1) * half]
            out[q * half : (q + 1) * half, cols] = update.astype(jnp.bfloat16)

    phase("drain")
    rs_all().wait_send()
    ag_all().wait_send()
    for copy in lat_first + lat_relays + w_first + w_relays + w_sent:
        copy.wait_send()
    for d in range(1, sp_n):
        ctx_copy(d).wait_send()
    for q in range(2):
        pl.when(sp + 1 < sp_n)(lambda: kv_own(sp + 1, 0, q).wait_send())
        pl.when(sp > 0)(lambda: kv_own(sp - 1, 1, q).wait_send())
    for ok, copy in sent:
        pl.when(ok)(copy.wait_send)
    for d in range(1, tp_n):
        at_copy(d).wait_send()
    phase(None)


def fused(
    axes, latent, condition, context, context_vector, modulator, norm_gain, query_weight,
    key_weight, value_weight, head_gain, lambdas, context_bias, out_weight,
):
    sp_n, tp_n, dp_n = axes
    n = sp_n * tp_n
    rows, width = latent.shape[1:]
    half = rows // 2
    chunk = modulator.shape[1] // n
    ctx_rows = context.shape[1]
    qw = query_weight.shape[1]
    value = value_weight.shape[1]
    qrows = rows * tp_n
    wrows = out_weight.shape[0] // 4
    bf, f32 = jnp.bfloat16, jnp.float32
    vm = pl.BlockSpec(memory_space=pltpu.VMEM)
    hb = pl.BlockSpec(memory_space=pltpu.HBM)
    dma = lambda k: pltpu.SemaphoreType.DMA((k,))
    result = pl.pallas_call(
        functools.partial(fused_kernel, sp_n, tp_n, (qw // 2) ** (-0.5)),
        out_shape=pltpu.VMEM((rows, width), bf),
        in_specs=[hb] * 13,
        out_specs=vm,
        scratch_shapes=[
            pltpu.VMEM(condition.shape, bf),
            pltpu.VMEM((1, context_vector.shape[0]), bf),
            pltpu.VMEM((1, width), f32),
            pltpu.VMEM((1, value), f32),
            pltpu.VMEM((1, 1), f32),
            pltpu.VMEM(context_bias.shape, f32),
            pltpu.VMEM(modulator.shape, bf),
            pltpu.VMEM((n, 2, chunk), f32),
            pltpu.VMEM((n, 2, chunk), f32),
            pltpu.VMEM((n, 2, chunk), f32),
            pltpu.VMEM((tp_n * 2, half, width), bf),
            pltpu.VMEM((sp_n, ctx_rows, width), bf),
            pltpu.VMEM((width, qw), bf),
            pltpu.VMEM((width, qw + value), bf),
            pltpu.VMEM((tp_n * 4, wrows, width), bf),
            pltpu.VMEM((8, width), f32),
            pltpu.VMEM((qrows + sp_n * ctx_rows, width), bf),
            pltpu.VMEM((sp_n * 2, qrows // 2, qw + value), bf),
            pltpu.VMEM((tp_n, rows, value), bf),
            pltpu.VMEM((tp_n, rows, value), bf),
            dma(7), dma(6), dma(1), dma(1), dma(1), dma(1), dma(6), dma(6), dma(sp_n), dma(sp_n),
            dma(4), dma(sp_n * 2), dma(sp_n * 2), dma(6), dma(6), dma(6), dma(6), dma(tp_n), dma(tp_n),
        ],
        compiler_params=pltpu.CompilerParams(
            collective_id=0, has_side_effects=True, vmem_limit_bytes=66700000
        ),
        name="fused_block",
    )(
        latent.reshape(2, half, width),
        condition,
        context[0],
        context_vector[None, :],
        modulator,
        norm_gain[None, :],
        query_weight,
        key_weight,
        value_weight,
        head_gain[None, :],
        lambdas[None, :],
        context_bias,
        out_weight.reshape(4, wrows, width),
    )
    return result[None]


def choose(axes, *arrays):
    sp_n, tp_n, dp_n = axes
    latent, modulator, query_weight, value_weight = arrays[0], arrays[4], arrays[6], arrays[8]
    lambdas, out_weight = arrays[10], arrays[12]
    fits = (
        tp_n == 4
        and dp_n == 2
        and 1 < sp_n <= 8
        and lambdas.shape[0] == 1
        and query_weight.shape[1] == LANES
        and value_weight.shape[1] == LANES
        and modulator.shape[1] % (sp_n * tp_n * LANES) == 0
        and latent.shape[1] % 32 == 0
        and latent.shape[2] % 512 == 0
        and out_weight.shape[0] % 64 == 0
    )
    return fused(axes, *arrays) if fits else body(*arrays)


def solution(mesh):
    placed = (
        P("dp", ("sp", "tp"), None),
        P("dp", ("sp", "tp")),
        P("dp", "sp", None),
        P(("sp", "tp")),
        P(("sp", "tp"), None),
        P(),
        P(None, "tp"),
        P(None, "tp"),
        P(None, "tp"),
        P(),
        P("tp"),
        P("tp", None),
        P("tp", None),
    )
    axes = (mesh.shape["sp"], mesh.shape["tp"], mesh.shape["dp"])
    return jax.shard_map(
        functools.partial(choose, axes), mesh=mesh, in_specs=placed, out_specs=P("dp", ("sp", "tp"), None), check_vma=False
    )
```

profile of v0, /device:TPU:0, one launch (start us, length us, event | category | flops | bytes accessed | tf_op | source)
XLA Modules:
  0.0 34.8 jit_solution(13135175720160012185)
XLA Ops:
  0.7 33.5 %fused_block.1 = bf16[64,2048]{1,0:T(8,128)(2,1)S(1)} custom-call(bf16[2,32,2048]{2,1,0:T(8,128)(2,1)} %bitcast.11, bf16[1,128]{1,0:T(2,128)(2,1)} %condition_in.1, bf16[8,2048]{1,0:T(8,128)(2,1)} %bitcast.12, bf16[1,128]{1,0:T(2,128)(2,1)} %bitcast.14, bf16[128,6144]{1,0:T(8,128)(2,1)} %modulator.1, f32[1,2048]{1,0:T(1,128)} %bitcast.13, ...), custom_call_target="tpu_custom_call" | custom-call | tf_op jit(solution)/shard_map/fused_block/pallas_call | solution.py:652
  34.1 0.7 %copy.15 = bf16[1,64,2048]{2,1,0:T(8,128)(2,1)} copy(bf16[1,64,2048]{2,1,0:T(8,128)(2,1)S(1)} %bitcast.9) | data formatting | bytes 524288
where the time goes:
time: 35 us; the launch traced here: 34.8 us
  Pallas kernels  33.5 us (96%)
  local copies, waits for them, and re-layouts  0.71 us (2%)
  between operations  0.66 us (2%)
    pallas_call x1, Pallas kernels, fused(): pl.pallas_call(functools.partial(fused_kernel, sp_n, tp_n, (qw // 2) ** (...  33.5 us
    unnamed x1, local copies, waits for them, and re-layouts  0.71 us

commit v1 on v0

v1 whole, which is shorter than its diff:
```python
import functools

import jax
import jax.numpy as jnp
from jax import lax
from jax.experimental import pallas as pl
from jax.experimental.pallas import tpu as pltpu
from jax.sharding import PartitionSpec as P

EPSILON = 1e-06
OUT_SCALE = 0.8
KEY_BLOCK = 2048
LOW_START = -1e30


def modulate(inputs, gain_vector, shift_vector, scale_vector):
    as_float = inputs.astype(jnp.float32)
    normed = as_float * lax.rsqrt(jnp.mean(as_float * as_float, axis=-1, keepdims=True) + EPSILON)
    return (normed * gain_vector * (1.0 + scale_vector) + shift_vector).astype(jnp.bfloat16)


def fold_block(running, queries, keys_in, values_in, key_flags, bias_table, score_scale):
    run_max, run_total, summed = running
    scores = (
        jnp.einsum("qhmd,khmd->hmqk", queries, keys_in, preferred_element_type=jnp.float32)
        * score_scale
    )
    if key_flags is not None:
        scores = scores + bias_table[:, :, None, None] * key_flags
    new_max = jnp.maximum(run_max, jnp.max(scores, axis=-1))
    shrink = jnp.exp(run_max - new_max)
    weights = jnp.exp(scores - new_max[..., None])
    run_total = run_total * shrink + jnp.sum(weights, axis=-1)
    summed = summed * shrink[..., None] + jnp.einsum(
        "hmqk,khe->hmqe",
        weights.astype(jnp.bfloat16),
        values_in,
        preferred_element_type=jnp.float32,
    )
    return (new_max, run_total, summed)


def fold_keys(running, queries, keys_in, values_in, key_flags, bias_table, score_scale):
    full_blocks = keys_in.shape[0] // KEY_BLOCK
    if full_blocks > 1:
        edge = full_blocks * KEY_BLOCK
        stacked = (
            keys_in[:edge].reshape((full_blocks, KEY_BLOCK) + keys_in.shape[1:]),
            values_in[:edge].reshape((full_blocks, KEY_BLOCK) + values_in.shape[1:]),
        )
        if key_flags is not None:
            stacked = stacked + (key_flags[:edge].reshape(full_blocks, KEY_BLOCK),)

        def fold_step(current, block_data):
            flag_part = None if key_flags is None else block_data[2]
            return (
                fold_block(
                    current,
                    queries,
                    block_data[0],
                    block_data[1],
                    flag_part,
                    bias_table,
                    score_scale,
                ),
                None,
            )

        running, ignored = lax.scan(fold_step, running, stacked)
        keys_in = keys_in[edge:]
        values_in = values_in[edge:]
        key_flags = None if key_flags is None else key_flags[edge:]
    if keys_in.shape[0] > 0:
        running = fold_block(
            running, queries, keys_in, values_in, key_flags, bias_table, score_scale
        )
    return running


def body(
    latent,
    condition,
    context,
    context_vector,
    modulator,
    norm_gain,
    query_weight,
    key_weight,
    value_weight,
    head_gain,
    lambdas,
    context_bias,
    out_weight,
):
    model_width = latent.shape[2]
    local_heads = lambdas.shape[0]
    query_width = query_weight.shape[1]
    head_size = query_width // (2 * local_heads)
    value_size = value_weight.shape[1] // local_heads
    score_scale = head_size ** (-0.5)
    activated = jax.nn.silu(
        jnp.concatenate([condition, context_vector[None, :]], axis=0).astype(jnp.float32)
    )
    partial_terms = jnp.dot(
        activated.astype(jnp.bfloat16), modulator, preferred_element_type=jnp.float32
    )
    modulations = lax.psum(partial_terms, ("sp", "tp"))
    hidden = modulate(
        latent[0],
        norm_gain,
        modulations[0, :model_width],
        modulations[0, model_width : 2 * model_width],
    )
    ctx_hidden = modulate(
        context[0],
        norm_gain,
        modulations[1, :model_width],
        modulations[1, model_width : 2 * model_width],
    )
    gate_vector = modulations[0, 2 * model_width :]
    incoming = lax.all_gather(hidden, "tp", axis=0, tiled=True)
    projected = jnp.concatenate(
        [
            jnp.dot(incoming, query_weight, preferred_element_type=jnp.float32),
            jnp.dot(incoming, key_weight, preferred_element_type=jnp.float32),
            jnp.dot(incoming, value_weight, preferred_element_type=jnp.float32),
        ],
        axis=1,
    ).astype(jnp.bfloat16)
    query_rows = projected.shape[0]
    queries = projected[:, :query_width].reshape(query_rows, local_heads, 2, head_size)
    own_keys = projected[:, query_width : 2 * query_width]
    own_values = projected[:, 2 * query_width :]
    gathered_context = lax.all_gather(ctx_hidden, "sp", axis=0, tiled=True)
    ctx_keys = jnp.dot(gathered_context, key_weight, preferred_element_type=jnp.float32).astype(
        jnp.bfloat16
    )
    ctx_values = jnp.dot(gathered_context, value_weight, preferred_element_type=jnp.float32).astype(
        jnp.bfloat16
    )
    start_carry = (
        jnp.full((local_heads, 2, query_rows), LOW_START, jnp.float32),
        jnp.zeros((local_heads, 2, query_rows), jnp.float32),
        jnp.zeros((local_heads, 2, query_rows, value_size), jnp.float32),
    )
    pieces = (own_keys, own_values)
    initial = fold_keys(
        start_carry,
        queries,
        ctx_keys.reshape(-1, local_heads, 2, head_size),
        ctx_values.reshape(-1, local_heads, value_size),
        jnp.ones((ctx_keys.shape[0],), jnp.float32),
        context_bias,
        score_scale,
    )
    incoming = (
        lax.all_gather(pieces[0], "sp", axis=0, tiled=True),
        lax.all_gather(pieces[1], "sp", axis=0, tiled=True),
    )
    run_max, run_total, summed = fold_keys(
        initial,
        queries,
        incoming[0].reshape(-1, local_heads, 2, head_size),
        incoming[1].reshape(-1, local_heads, value_size),
        None,
        context_bias,
        score_scale,
    )
    mixed = (
        summed[:, 0] / run_total[:, 0, :, None]
        - lambdas[:, None, None] * summed[:, 1] / run_total[:, 1, :, None]
    )
    normed = (
        mixed
        * lax.rsqrt(jnp.mean(mixed * mixed, axis=-1, keepdims=True) + EPSILON)
        * head_gain
        * OUT_SCALE
    )
    attended = (
        jnp.transpose(normed, (1, 0, 2))
        .reshape(query_rows, local_heads * value_size)
        .astype(jnp.bfloat16)
    )
    exchanged = lax.all_to_all(attended, "tp", split_axis=0, concat_axis=1, tiled=True)
    whole_weight = lax.all_gather(out_weight, "tp", axis=0, tiled=True)
    branch = jnp.dot(exchanged, whole_weight, preferred_element_type=jnp.float32)
    result = (latent[0].astype(jnp.float32) + gate_vector * branch).astype(jnp.bfloat16)
    return result[None]


MESH = pl.DeviceIdType.MESH
LANES = 128


class Phases:
    def __init__(self):
        self.open = None

    def __call__(self, name):
        if self.open is not None:
            self.open.__exit__(None, None, None)
        self.open = None
        if name is not None:
            self.open = jax.named_scope(name)
            self.open.__enter__()


def fused_kernel(
    sp_n, tp_n, score_scale,
    latent, condition_in, context, vector_in, modulator, gain_in,
    query_weight, key_weight, value_weight, head_gain_in, lambdas_in, bias_in, out_weight,
    out,
    condition, context_vector, norm_gain, head_gain, lambdas, context_bias,
    mod_v, gate_v, fast_p, fast_z, slow_z, slow_p, lat, ctx, w_qkv, w_out, vecs, hid, kvb, ckv,
    att_out, att_in, acc,
    small_sem, own_sem, mod_sem, two_sem, far_sem, fp_ss, fp_rs, fz_ss, fz_rs, sz_ss, sz_rs, sl_ss, sl_rs,
    lat_ss, lat_rs, ck_ss, ck_rs, kv_ss, kv_rs, wt_ss, wt_rs, wd_ss, wd_rs, at_ss, at_rs,
):
    sp = lax.axis_index("sp")
    tp = lax.axis_index("tp")
    dp = lax.axis_index("dp")
    across = tp + 1 - 2 * lax.rem(tp, 2)
    along = lax.rem(tp + 2, 4)
    corner = along + 1 - 2 * lax.rem(along, 2)
    roles = (tp, across, along, corner)
    half = lat.shape[1]
    width = lat.shape[2]
    rows = half * 2
    qrows = rows * tp_n
    depth = gate_v.shape[0]
    ctx_rows = ctx.shape[0]
    high = (2 * sp) // sp_n

    def z_peer(t):
        up = (t - 1) + jnp.where(t - 1 >= sp, 1, 0)
        down = (sp_n - t) - jnp.where(sp_n - t <= sp, 1, 0)
        return jnp.where(high == 0, up, down)

    phase = Phases()
    phase("enter")
    barrier = pltpu.get_barrier_semaphore()

    def greet(where):
        pl.semaphore_signal(barrier, inc=1, device_id=where, device_id_type=MESH)

    has_up, has_down = sp + 1 < sp_n, sp > 0
    middle = jnp.logical_and(has_up, has_down)
    for peer in (across, along, corner):
        greet((sp, peer, dp))
    pl.when(has_up)(lambda: greet((sp + 1, tp, dp)))
    pl.when(has_down)(lambda: greet((sp - 1, tp, dp)))
    greet((sp, tp, 1 - dp))

    small = [
        pltpu.make_async_copy(source, place, small_sem.at[k])
        for k, (source, place) in enumerate((
            (condition_in, condition), (vector_in, context_vector), (context, ctx),
            (gain_in, norm_gain), (head_gain_in, head_gain), (lambdas_in, lambdas),
            (bias_in, context_bias),
        ))
    ]
    cut = width // MOD_CUTS

    def mod_loads(k):
        return [
            pltpu.make_async_copy(
                modulator.at[:, pl.ds(part * width + k * cut, cut)], mod_v.at[part, :, pl.ds(k * cut, cut)],
                mod_sem.at[k],
            )
            for part in range(2)
        ]

    def here(place, sem):
        return pltpu.make_async_copy(place, place, sem)

    loads = [
        pltpu.make_async_copy(latent, lat.at[pl.ds(tp * 2, 2)], own_sem.at[0]),
        pltpu.make_async_copy(modulator.at[:, pl.ds(2 * width, width)], gate_v, own_sem.at[1]),
        pltpu.make_async_copy(key_weight, w_qkv.at[:, pl.ds(0, LANES)], own_sem.at[2]),
        pltpu.make_async_copy(value_weight, w_qkv.at[:, pl.ds(LANES, LANES)], own_sem.at[2]),
        pltpu.make_async_copy(query_weight, w_qkv.at[:, pl.ds(2 * LANES, LANES)], own_sem.at[2]),
        pltpu.make_async_copy(out_weight, w_out.at[pl.ds(tp * 4, 4)], own_sem.at[3]),
    ]
    for load in small[:2]:
        load.start()
    for k in range(MOD_CUTS):
        for load in mod_loads(k):
            load.start()

    phase("partial")
    for load in small[:2]:
        load.wait()
    rows_in = jnp.concatenate([condition[...], context_vector[...]], axis=0).astype(jnp.float32)
    activated = jax.nn.silu(rows_in).astype(jnp.bfloat16)
    own_act, ctx_act = activated[0:1], activated[1:2]
    blank = jnp.zeros_like(own_act)
    left = jnp.concatenate([own_act, blank, ctx_act, blank], axis=0)
    right = jnp.concatenate([blank, own_act, blank, ctx_act], axis=0)
    stacked = jnp.concatenate([left, right], axis=1)
    for load in loads[:2] + small[2:] + loads[2:]:
        load.start()
    for k in range(MOD_CUTS):
        cols = slice(k * cut, (k + 1) * cut)
        here(mod_v.at[:, :, pl.ds(k * cut, cut)], mod_sem.at[k]).wait()
        terms = jnp.dot(
            stacked, mod_v[:, :, cols].reshape(2 * depth, cut), preferred_element_type=jnp.float32
        ).astype(jnp.bfloat16)
        fast_p[tp, :, cols] = terms[0:2]
        slow_z[sp, 0:2, cols] = terms[2:4]

    phase("barrier")
    pl.semaphore_wait(barrier, jnp.where(middle, 6, 5))

    def vouch(sem, where):
        pl.semaphore_signal(sem, inc=1, device_id=where, device_id_type=MESH)

    def vouch_both():
        vouch(two_sem, (sp + 1, tp, dp))
        vouch(two_sem, (sp - 1, tp, dp))

    pl.when(middle)(vouch_both)
    phase("sends")


    def plane_copy(buf, d, ss, rs):
        return pltpu.make_async_remote_copy(
            src_ref=buf.at[tp], dst_ref=buf.at[tp], send_sem=ss, recv_sem=rs,
            device_id=(sp, roles[d], dp), device_id_type=MESH,
        )

    def z_copy(buf, t, ss, rs):
        return pltpu.make_async_remote_copy(
            src_ref=buf.at[sp], dst_ref=buf.at[sp], send_sem=ss, recv_sem=rs,
            device_id=(z_peer(t), tp, dp), device_id_type=MESH,
        )

    def some(place, ss, rs):
        return pltpu.make_async_remote_copy(
            src_ref=place, dst_ref=place, send_sem=ss, recv_sem=rs,
            device_id=(sp, across, dp), device_id_type=MESH,
        )

    def three(buf, ss, rs):
        return some(buf.at[pl.ds(0, 3)], ss, rs)

    for d in (3, 1, 2):
        plane_copy(fast_p, d, fp_ss, fp_rs).start()
    phase("lat_first")

    class Plane:
        def __init__(self, buf, index, ss, rs):
            self.buf, self.index, self.ss, self.rs = buf, index, ss, rs

        def copy(self, owner, part_no, target, kind):
            place = self.buf.at[self.index(owner, part_no)]
            return pltpu.make_async_remote_copy(
                src_ref=place, dst_ref=place, send_sem=self.ss,
                recv_sem=self.rs.at[kind * 2 + part_no],
                device_id=(sp, target, dp), device_id_type=MESH,
            )

        def first(self):
            return [
                self.copy(tp, 0, across, 0),
                self.copy(tp, 1, along, 1),
                self.copy(tp, 1, across, 0),
                self.copy(tp, 0, along, 1),
            ]

        def relays(self):
            return [self.copy(across, 0, along, 2), self.copy(along, 1, across, 2)]

        def arrival(self, kind, part_no):
            owner = (across, along, corner)[kind]
            return self.copy(owner, part_no, across, kind)

    plane = Plane(lat, lambda o, q: o * 2 + q, lat_ss, lat_rs)
    loads[0].wait()
    for copy in plane.first():
        copy.start()

    loads[1].wait()
    gate_rows = jnp.concatenate([own_act, blank], axis=0)
    slow_z[sp, 2:4] = jnp.dot(gate_rows, gate_v[...], preferred_element_type=jnp.float32).astype(jnp.bfloat16)
    phase("slow_send")
    z_copy(slow_z, 1, sz_ss, sz_rs).start()
    pl.semaphore_wait(two_sem, 1)
    pl.when(middle)(lambda: vouch(far_sem, (jnp.where(high == 0, sp - 1, sp + 1), tp, dp)))
    z_copy(slow_z, 2, sz_ss, sz_rs).start()
    pl.when(jnp.logical_not(middle))(lambda: pl.semaphore_wait(far_sem, 1))
    z_copy(slow_z, 3, sz_ss, sz_rs).start()

    def row_scale(at):
        x = lat[at].astype(jnp.float32)
        return lax.rsqrt(jnp.mean(x * x, axis=-1, keepdims=True) + EPSILON)

    scales = {}

    def measure(role, q):
        scales[role, q] = row_scale(roles[role] * 2 + q)

    def total_of(buf, count):
        total = buf[0].astype(jnp.float32)
        for p in range(1, count):
            total = total + buf[p].astype(jnp.float32)
        return total

    for q in range(2):
        measure(0, q)
    phase("plane_wait")
    three(fast_p, fp_ss, fp_rs).wait_recv()
    fast_z[sp] = total_of(fast_p, tp_n).astype(jnp.bfloat16)
    for t in (3, 2, 1):
        z_copy(fast_z, t, fz_ss, fz_rs).start()

    phase("lat_relay")
    relays = plane.relays()
    plane.arrival(0, 0).wait_recv()
    relays[0].start()
    plane.arrival(1, 1).wait_recv()
    relays[1].start()
    measure(1, 0)
    measure(2, 1)
    phase("slow_relay")
    three(slow_z, sz_ss, sz_rs).wait_recv()
    slow_p[tp] = total_of(slow_z, sp_n).astype(jnp.bfloat16)
    for d in (3, 1, 2):
        plane_copy(slow_p, d, sl_ss, sl_rs).start()
    loads[5].wait()
    wplane = Plane(w_out, lambda o, q: o * 4 + dp * 2 + q, wt_ss, wt_rs)
    for copy in wplane.first():
        copy.start()
    for load in small[2:]:
        load.wait()
    here(w_qkv, own_sem.at[2]).wait()

    phase("z_wait")
    three(fast_z, fz_ss, fz_rs).wait_recv()
    fast = total_of(fast_z, sp_n)
    gain = norm_gain[...]
    vecs[0:1, :] = gain * (1.0 + fast[1:2])
    vecs[1:2, :] = fast[0:1]

    def norm_role(role):
        for q in range(2):
            at = (role * 2 + q) * half
            x = lat[roles[role] * 2 + q].astype(jnp.float32)
            hid[at : at + half, :] = (x * scales[role, q] * vecs[0:1, :] + vecs[1:2, :]).astype(jnp.bfloat16)

    def kv_copy(block, q, to):
        place = kvb.at[q * sp_n + block]
        spread = jnp.abs(to - block)
        end = jnp.logical_or(to == 0, to == sp_n - 1)
        far = jnp.logical_or(spread == sp_n - 1, jnp.logical_and(spread == 2, jnp.logical_not(end)))
        slot = RELAYED if q == RELAYED else jnp.where(far, q, RELAYED + 1)
        return pltpu.make_async_remote_copy(
            src_ref=place, dst_ref=place, send_sem=kv_ss, recv_sem=kv_rs.at[slot],
            device_id=(to, tp, dp), device_id_type=MESH,
        )

    def kv_wait(count, slot):
        return some(kvb.at[pl.ds(0, count)], kv_ss, kv_rs.at[slot])

    def kv_rows(first, last):
        product = jnp.dot(hid[first:last, :], w_qkv[:, : 2 * LANES], preferred_element_type=jnp.float32)
        return product.astype(jnp.bfloat16)

    def kv_send(q):
        far = kv_copy(sp, q, z_peer(3))
        if q < RELAYED:
            pl.when(middle)(far.start)
        else:
            far.start()
        for t in (2, 1):
            kv_copy(sp, q, z_peer(t)).start()

    def kv_role(q):
        kvb[q * sp_n + sp] = kv_rows(q * rows, (q + 1) * rows)
        kv_send(q)

    def relay(q):
        def act():
            kv_wait(1, q).wait_recv()
            kv_copy(z_peer(3), q, jnp.where(high == 0, sp - 1, sp + 1)).start()

        pl.when(middle)(act)

    phase("kv_own")
    norm_role(0)
    kv_role(0)
    phase("kv_across")
    plane.arrival(0, 1).wait_recv()
    measure(1, 1)
    norm_role(1)
    kv_role(1)
    phase("kv_along")
    plane.arrival(1, 0).wait_recv()
    measure(2, 0)
    norm_role(2)
    kv_role(2)
    phase("kv_corner")
    for q in range(2):
        plane.arrival(2, q).wait_recv()
        measure(3, q)
    norm_role(3)
    kv_role(3)

    phase("queries")
    queries = jnp.dot(hid[:qrows, :], w_qkv[:, 2 * LANES :], preferred_element_type=jnp.float32) * score_scale
    queries = queries.astype(jnp.bfloat16)
    head = queries.shape[1] // 2
    lane = lax.broadcasted_iota(jnp.int32, queries.shape, 1)
    zero = jnp.zeros_like(queries)
    both = jnp.concatenate(
        [jnp.where(lane < head, queries, zero), jnp.where(lane < head, zero, queries)], axis=0
    )

    def score(keys):
        return lax.dot_general(
            both, keys, (((1,), (1,)), ((), ())), preferred_element_type=jnp.float32
        )

    map_row = lax.broadcasted_iota(jnp.int32, (2 * qrows, 1), 0)
    bias = jnp.where(map_row < qrows, context_bias[0:1, 0:1], context_bias[0:1, 1:2])

    def fold(running, scores, values):
        top = jnp.max(scores, axis=-1, keepdims=True)
        if running is not None:
            top = jnp.maximum(running[0], top)
        weights = jnp.exp(scores - top)
        count = jnp.sum(weights, axis=-1, keepdims=True)
        summed = jnp.dot(weights.astype(jnp.bfloat16), values, preferred_element_type=jnp.float32)
        if running is not None:
            shrink = jnp.exp(running[0] - top)
            count = running[1] * shrink + count
            summed = running[2] * shrink + summed
        return top, count, summed

    def fold_keys_in(running, places):
        block = jnp.concatenate([kvb[place] for place in places], axis=0)
        return fold(running, score(block[:, :LANES]), block[:, LANES:])

    def piece(t, q):
        return q * sp_n + (sp if t == 0 else z_peer(t))

    phase("fold_own")
    running = fold_keys_in(None, [piece(0, q) for q in range(tp_n)])
    phase("slow_wait")
    three(slow_p, sl_ss, sl_rs).wait_recv()
    slow = total_of(slow_p, tp_n)
    vecs[2:3, :] = gain * (1.0 + slow[1:2])
    vecs[3:4, :] = slow[0:1]
    vecs[4:5, :] = slow[2:3]
    cx = ctx[...].astype(jnp.float32)
    cx = cx * lax.rsqrt(jnp.mean(cx * cx, axis=-1, keepdims=True) + EPSILON)
    hid[qrows : qrows + ctx_rows, :] = (cx * vecs[2:3, :] + vecs[3:4, :]).astype(jnp.bfloat16)
    ckv[sp] = kv_rows(qrows, qrows + ctx_rows)
    for t in (1, 2, 3):
        z_copy(ckv, t, ck_ss, ck_rs).start()
    phase("relays")
    for q in range(RELAYED):
        relay(q)

    def sibling(owner, part_no):
        place = w_out.at[owner * 4 + dp * 2 + part_no]
        return pltpu.make_async_remote_copy(
            src_ref=place, dst_ref=place, send_sem=wd_ss, recv_sem=wd_rs,
            device_id=(sp, tp, 1 - dp), device_id_type=MESH,
        )

    owners = (across, along, corner)

    def swap(kind, part_no, wait=True):
        if wait:
            wplane.arrival(kind, part_no).wait_recv()
        sibling(owners[kind], part_no).start()

    phase("w_relay")
    w_relays = wplane.relays()
    wplane.arrival(0, 0).wait_recv()
    w_relays[0].start()
    wplane.arrival(1, 1).wait_recv()
    w_relays[1].start()
    swap(0, 0, False)
    swap(1, 1, False)
    phase("take_near")
    kv_wait(2 * RELAYED, RELAYED + 1).wait_recv()
    phase("fold_near")
    running = fold_keys_in(running, [piece(t, q) for t in (1, 2) for q in range(RELAYED)])
    phase("ctx")
    three(ckv, ck_ss, ck_rs).wait_recv()
    ctx_kv = ckv[...].reshape(sp_n * ctx_rows, 2 * LANES)
    running = fold(running, score(ctx_kv[:, :LANES]) + bias, ctx_kv[:, LANES:])
    phase("w_second")
    swap(0, 1)
    swap(1, 0)
    phase("take_far")
    for q in range(RELAYED):
        pl.when(jnp.logical_not(middle))(kv_wait(1, q).wait_recv)
    running = fold_keys_in(running, [piece(3, q) for q in range(RELAYED)])
    phase("take_last")
    kv_wait(3, RELAYED).wait_recv()
    phase("fold_last")
    running = fold_keys_in(running, [piece(t, RELAYED) for t in (1, 2, 3)])

    phase("finish")
    top, count, summed = running
    shares = summed / count
    mixed = shares[:qrows] - lambdas[...] * shares[qrows:]
    normed = (
        mixed
        * lax.rsqrt(jnp.mean(mixed * mixed, axis=-1, keepdims=True) + EPSILON)
        * head_gain[...]
        * OUT_SCALE
    ).astype(jnp.bfloat16)
    for p in range(tp_n):
        att_out[p] = normed[p * rows : (p + 1) * rows]

    def at_copy(d):
        return pltpu.make_async_remote_copy(
            src_ref=att_out.at[d], dst_ref=att_in.at[tp], send_sem=at_ss, recv_sem=at_rs.at[d // 2],
            device_id=(sp, roles[d], dp), device_id_type=MESH,
        )

    for d in (3, 1, 2):
        at_copy(d).start()
    att_in[tp] = att_out[0]

    phase("w_wait")
    swap(2, 0)
    swap(2, 1)
    some(w_out.at[pl.ds(0, 6)], wd_ss, wd_rs).wait_recv()

    def pair_terms(base, cols):
        pair = jnp.concatenate([att_in[base], att_in[base + 1]], axis=1)
        weight = w_out[pl.ds(base * 4, 8), :, cols].reshape(pair.shape[1], cols.stop - cols.start)
        return jnp.dot(pair, weight, preferred_element_type=jnp.float32)

    step = 512
    spans = [slice(first, first + step) for first in range(0, width, step)]
    phase("at_wait")
    some(att_in.at[pl.ds(0, 1)], at_ss, at_rs.at[0]).wait_recv()
    for cols in spans:
        acc[:, cols] = pair_terms(tp - lax.rem(tp, 2), cols)
    phase("at_wait2")
    some(att_in.at[pl.ds(0, 2)], at_ss, at_rs.at[1]).wait_recv()

    phase("out")
    for cols in spans:
        branch = acc[:, cols] + pair_terms(along - lax.rem(along, 2), cols)
        for q in range(2):
            mine = lat[tp * 2 + q, :, cols].astype(jnp.float32)
            update = mine + vecs[4:5, cols] * branch[q * half : (q + 1) * half]
            out[q * half : (q + 1) * half, cols] = update.astype(jnp.bfloat16)

    phase("drain")
    for buf, ss, rs in (
        (fast_p, fp_ss, fp_rs), (fast_z, fz_ss, fz_rs), (slow_z, sz_ss, sz_rs), (slow_p, sl_ss, sl_rs),
        (ckv, ck_ss, ck_rs), (att_out, at_ss, at_rs.at[0]),
    ):
        three(buf, ss, rs).wait_send()
    some(lat.at[pl.ds(0, 6)], lat_ss, lat_rs.at[0]).wait_send()
    some(w_out.at[pl.ds(0, 6)], wt_ss, wt_rs.at[0]).wait_send()
    some(w_out.at[pl.ds(0, 6)], wd_ss, wd_rs).wait_send()
    pl.when(middle)(kv_wait(tp_n * 3 + RELAYED, 0).wait_send)
    pl.when(jnp.logical_not(middle))(kv_wait(tp_n * 3 - RELAYED, 0).wait_send)
    phase(None)


RELAYED = 3
MOD_CUTS = 4


def fused(
    axes, latent, condition, context, context_vector, modulator, norm_gain, query_weight,
    key_weight, value_weight, head_gain, lambdas, context_bias, out_weight,
):
    sp_n, tp_n, dp_n = axes
    rows, width = latent.shape[1:]
    half = rows // 2
    depth = modulator.shape[0]
    ctx_rows = context.shape[1]
    qw = query_weight.shape[1]
    value = value_weight.shape[1]
    qrows = rows * tp_n
    wrows = out_weight.shape[0] // 4
    bf, f32 = jnp.bfloat16, jnp.float32
    vm = pl.BlockSpec(memory_space=pltpu.VMEM)
    hb = pl.BlockSpec(memory_space=pltpu.HBM)
    dma = lambda k: pltpu.SemaphoreType.DMA((k,))
    result = pl.pallas_call(
        functools.partial(fused_kernel, sp_n, tp_n, (qw // 2) ** (-0.5)),
        out_shape=pltpu.VMEM((rows, width), bf),
        in_specs=[hb] * 13,
        out_specs=vm,
        scratch_shapes=[
            pltpu.VMEM(condition.shape, bf),
            pltpu.VMEM((1, context_vector.shape[0]), bf),
            pltpu.VMEM((1, width), f32),
            pltpu.VMEM((1, value), f32),
            pltpu.VMEM((1, 1), f32),
            pltpu.VMEM(context_bias.shape, f32),
            pltpu.VMEM((2, depth, width), bf),
            pltpu.VMEM((depth, width), bf),
            pltpu.VMEM((tp_n, 2, width), bf),
            pltpu.VMEM((sp_n, 2, width), bf),
            pltpu.VMEM((sp_n, 4, width), bf),
            pltpu.VMEM((tp_n, 4, width), bf),
            pltpu.VMEM((tp_n * 2, half, width), bf),
            pltpu.VMEM((ctx_rows, width), bf),
            pltpu.VMEM((width, 2 * qw + value), bf),
            pltpu.VMEM((tp_n * 4, wrows, width), bf),
            pltpu.VMEM((8, width), f32),
            pltpu.VMEM((qrows + ctx_rows, width), bf),
            pltpu.VMEM((sp_n * tp_n, rows, qw + value), bf),
            pltpu.VMEM((sp_n, ctx_rows, qw + value), bf),
            pltpu.VMEM((tp_n, rows, value), bf),
            pltpu.VMEM((tp_n, rows, value), bf),
            pltpu.VMEM((rows, width), f32),
            dma(7), dma(4), dma(MOD_CUTS), *[pltpu.SemaphoreType.REGULAR] * 2,
            *[pltpu.SemaphoreType.DMA] * 8, pltpu.SemaphoreType.DMA, dma(6), pltpu.SemaphoreType.DMA,
            pltpu.SemaphoreType.DMA, pltpu.SemaphoreType.DMA, dma(RELAYED + 2), pltpu.SemaphoreType.DMA, dma(6),
            pltpu.SemaphoreType.DMA, pltpu.SemaphoreType.DMA, pltpu.SemaphoreType.DMA, dma(2),
        ],
        compiler_params=pltpu.CompilerParams(
            collective_id=0, has_side_effects=True, vmem_limit_bytes=66700000
        ),
        name="fused_block",
    )(
        latent.reshape(2, half, width),
        condition,
        context[0],
        context_vector[None, :],
        modulator,
        norm_gain[None, :],
        query_weight,
        key_weight,
        value_weight,
        head_gain[None, :],
        lambdas[None, :],
        context_bias,
        out_weight.reshape(4, wrows, width),
    )
    return result[None]


def choose(axes, *arrays):
    sp_n, tp_n, dp_n = axes
    latent, modulator, query_weight, value_weight = arrays[0], arrays[4], arrays[6], arrays[8]
    lambdas, out_weight, context = arrays[10], arrays[12], arrays[2]
    fits = (
        tp_n == 4
        and dp_n == 2
        and sp_n == 4
        and lambdas.shape[0] == 1
        and query_weight.shape[1] == LANES
        and value_weight.shape[1] == LANES
        and modulator.shape[1] == 3 * latent.shape[2]
        and modulator.shape[0] % LANES == 0
        and context.shape[1] % 8 == 0
        and latent.shape[1] % 32 == 0
        and latent.shape[2] % 512 == 0
        and out_weight.shape[0] % 64 == 0
    )
    return fused(axes, *arrays) if fits else body(*arrays)


def solution(mesh):
    placed = (
        P("dp", ("sp", "tp"), None),
        P("dp", ("sp", "tp")),
        P("dp", "sp", None),
        P(("sp", "tp")),
        P(("sp", "tp"), None),
        P(),
        P(None, "tp"),
        P(None, "tp"),
        P(None, "tp"),
        P(),
        P("tp"),
        P("tp", None),
        P("tp", None),
    )
    axes = (mesh.shape["sp"], mesh.shape["tp"], mesh.shape["dp"])
    return jax.shard_map(
        functools.partial(choose, axes), mesh=mesh, in_specs=placed, out_specs=P("dp", ("sp", "tp"), None), check_vma=False
    )
```

time: 35 us -> 30.5 us (0.87)
  Pallas kernels: 33.5 us -> 29 us
    pallas_call x1, Pallas kernels: 33.5 us -> 29 us  [fused(): pl.pallas_call(functools.partial(fused_kernel, sp_n, tp_n, (qw // 2) ** (...]
where the time goes in v1:
time: 30.5 us; the launch traced here: 30.4 us
  Pallas kernels  29 us (95%)
  local copies, waits for them, and re-layouts  0.71 us (2%)
  between operations  0.66 us (2%)
    pallas_call x1, Pallas kernels, fused(): pl.pallas_call(functools.partial(fused_kernel, sp_n, tp_n, (qw // 2) ** (...  29 us
    unnamed x1, local copies, waits for them, and re-layouts  0.71 us

profile of v1, /device:TPU:0, one launch (start us, length us, event | category | flops | bytes accessed | tf_op | source)
XLA Modules:
  0.0 30.4 jit_solution(9773747838921890658)
XLA Ops:
  0.7 29.0 %fused_block.1 = bf16[64,2048]{1,0:T(8,128)(2,1)S(1)} custom-call(bf16[2,32,2048]{2,1,0:T(8,128)(2,1)} %bitcast.11, bf16[1,128]{1,0:T(2,128)(2,1)} %condition_in.1, bf16[8,2048]{1,0:T(8,128)(2,1)} %bitcast.12, bf16[1,128]{1,0:T(2,128)(2,1)} %bitcast.14, bf16[128,6144]{1,0:T(8,128)(2,1)} %modulator.1, f32[1,2048]{1,0:T(1,128)} %bitcast.13, ...), custom_call_target="tpu_custom_call" | custom-call | tf_op jit(solution)/shard_map/fused_block/pallas_call | solution.py:691
  29.7 0.7 %copy.15 = bf16[1,64,2048]{2,1,0:T(8,128)(2,1)} copy(bf16[1,64,2048]{2,1,0:T(8,128)(2,1)S(1)} %bitcast.9) | data formatting | bytes 524288
